TPU v7x, 32 devices: a whole 2x2x4 slice. The times are simulated.
32 devices in a mesh: dp: 4 (over y, x), kv: 4 (over z), tp: 2 (over core).
Axes of the slice: x: 2, y: 2, z: 4, core: 2. Of those that a mesh axis runs over, the one named last changes fastest.
Arguments:
- tokens: bfloat16 [32, 4096], P('dp', ('kv', 'tp')), as said below
- query_weight: bfloat16 [4096, 16, 128], P(None, 'tp', 'kv'), may hold values from -0.09375 to 0.09375
- key_weight: bfloat16 [4096, 16, 128], P(None, 'tp', 'kv'), may hold values from -0.09375 to 0.09375
- value_weight: bfloat16 [4096, 16, 256], P(None, 'tp', 'kv'), may hold values from -0.09375 to 0.09375
- gate_weight: bfloat16 [4096, 16, 256], P(None, 'tp', 'kv'), may hold values from -0.09375 to 0.09375
- decay_weight: bfloat16 [4096, 16, 128], P(None, 'tp', 'kv'), may hold values from -0.09375 to 0.09375
- decay_bias: float32 [16, 128], P('tp'), may hold values from -8 to 2
- states: float32 [32, 16, 128, 256], P(('dp', 'kv'), 'tp'), may hold values from -4 to 4
- head_gain: float32 [16, 256], P('tp'), may hold values from 0.1 to 1.9
- out_weight: bfloat16 [4096, 4096], P(None, ('kv', 'tp')), as said below
- norm1_gain: float32 [4096], P(('kv', 'tp')), may hold values from 0.1 to 1.9
- norm1_bias: float32 [4096], P(('kv', 'tp')), may hold values from -3 to 3
- up_weight: bfloat16 [4096, 16384], P(None, ('kv', 'tp')), may hold values from -0.09375 to 0.09375
- down_weight: bfloat16 [16384, 4096], P(('kv', 'tp')), as said below
- norm2_gain: float32 [4096], P(('kv', 'tp')), may hold values from 0.1 to 1.9
- norm2_bias: float32 [4096], P(('kv', 'tp')), may hold values from -3 to 3
Outputs:
- layer_out: bfloat16 [32, 4096], P('dp', ('kv', 'tp'))
- new_states: float32 [32, 16, 128, 256], P(('dp', 'kv'), 'tp')
Inputs may be any that keep to these rules, and one draw needn't show every extreme that they name: `tokens`: each block of 64 features has its own scale. `out_weight`: entries lie within 13 / sqrt(4096) of zero. `down_weight`: entries lie within 14 / sqrt(16384) of zero.
All inputs are finite; a program needn't handle non-finite values.
Results may differ from a plain program's by a relative error of at most 0.009.
Values may be sent and summed in bfloat16 or wider, within the bound.
A program may use at most 128 MiB of HBM per device.

v0:
```python
import jax
import jax.numpy as jnp
from jax import lax
from jax.sharding import PartitionSpec as P

D = 4096
KEY_DIM = 128
ALPHA = 2.0**0.5
TAU = 16.0
LN_EPS = 1e-05
RMS_EPS = 1e-06


def project_flat(inputs, weight):
    flattened = weight.reshape(weight.shape[0], -1)
    return jnp.dot(inputs, flattened, preferred_element_type=jnp.float32).astype(jnp.bfloat16)


def normalize(inputs, average, spread, row_gain, row_shift):
    return ((inputs - average) * lax.rsqrt(spread + LN_EPS) * row_gain + row_shift).astype(
        jnp.bfloat16
    )


def body(
    tokens,
    query_weight,
    key_weight,
    value_weight,
    gate_weight,
    decay_weight,
    decay_bias,
    states,
    head_gain,
    out_weight,
    norm1_gain,
    norm1_bias,
    up_weight,
    down_weight,
    norm2_gain,
    norm2_bias,
):
    whole = lax.all_gather(tokens, ("kv", "tp"), axis=1, tiled=True)
    weights_list = (query_weight, key_weight, decay_weight, value_weight, gate_weight)
    packed = jnp.concatenate([project_flat(whole, weight) for weight in weights_list], axis=1)
    arrived = lax.all_to_all(packed, "kv", split_axis=0, concat_axis=0, tiled=True)
    groups = lax.axis_size("kv")
    seq_count = whole.shape[0] // groups
    local_heads = query_weight.shape[1]
    unpacked = []
    start = 0
    for weight in weights_list:
        channels = weight.shape[2]
        width = local_heads * channels
        block = arrived[:, start : start + width].reshape(groups, seq_count, local_heads, channels)
        block = block.transpose(1, 2, 0, 3).reshape(seq_count, local_heads, groups * channels)
        unpacked.append(block.astype(jnp.float32))
        start = start + width
    query_rows = unpacked[0] * KEY_DIM ** (-0.5)
    key_rows = unpacked[1]
    decay_rows = unpacked[2]
    value_rows = unpacked[3]
    gate_rows = unpacked[4]
    retain = jnp.exp(jax.nn.log_sigmoid(decay_rows + decay_bias) / TAU)
    new_states = retain[..., None] * states + key_rows[..., :, None] * value_rows[..., None, :]
    readout = jnp.einsum("shk,shkv->shv", query_rows, new_states, precision=lax.Precision.HIGHEST)
    readout = (
        readout
        * lax.rsqrt(jnp.mean(readout * readout, axis=-1, keepdims=True) + RMS_EPS)
        * head_gain
    )
    attended = (readout * jax.nn.silu(gate_rows)).astype(jnp.bfloat16)
    seq_count, local_heads, value_width = attended.shape
    flat_width = local_heads * value_width
    collected = lax.all_gather(
        attended.reshape(1, seq_count, flat_width), ("kv", "tp"), axis=0, tiled=True
    )
    halves = lax.axis_size("tp")
    collected = collected.reshape(-1, halves, seq_count, flat_width)
    columns = out_weight.shape[1]
    out_parts = out_weight.reshape(halves, flat_width, columns)
    mixed_heads = jnp.einsum(
        "atsc,tcd->asd", collected, out_parts, preferred_element_type=jnp.float32
    ).reshape(-1, columns)
    residual_one = ALPHA * tokens.astype(jnp.float32) + mixed_heads
    offset = lax.axis_index(("kv", "tp")) * columns
    totals = lax.psum(
        (
            jnp.sum(residual_one, axis=-1, keepdims=True),
            jnp.sum(residual_one * residual_one, axis=-1, keepdims=True),
        ),
        ("kv", "tp"),
    )
    average = totals[0] / D
    spread = totals[1] / D - average * average
    normed_own = normalize(residual_one, average, spread, norm1_gain, norm1_bias)
    normed = lax.all_gather(normed_own, ("kv", "tp"), axis=1, tiled=True)
    lifted = jnp.dot(normed, up_weight, preferred_element_type=jnp.float32)
    hidden = jnp.square(jax.nn.relu(lifted)).astype(jnp.bfloat16)
    mixer_term = jnp.dot(hidden, down_weight, preferred_element_type=jnp.float32)
    mixer_all = lax.psum(mixer_term, ("kv", "tp"))
    residual_two = ALPHA * normed.astype(jnp.float32) + mixer_all
    average = jnp.sum(residual_two, axis=-1, keepdims=True) / D
    spread = jnp.sum(residual_two * residual_two, axis=-1, keepdims=True) / D - average * average
    own_rows = lax.dynamic_slice_in_dim(residual_two, offset, columns, 1)
    layer_out = normalize(own_rows, average, spread, norm2_gain, norm2_bias)
    return (layer_out, new_states)


def solution(mesh):
    placed = (
        P("dp", ("kv", "tp")),
        P(None, "tp", "kv"),
        P(None, "tp", "kv"),
        P(None, "tp", "kv"),
        P(None, "tp", "kv"),
        P(None, "tp", "kv"),
        P("tp", None),
        P(("dp", "kv"), "tp", None, None),
        P("tp", None),
        P(None, ("kv", "tp")),
        P(("kv", "tp")),
        P(("kv", "tp")),
        P(None, ("kv", "tp")),
        P(("kv", "tp"), None),
        P(("kv", "tp")),
        P(("kv", "tp")),
    )
    return jax.shard_map(
        body,
        mesh=mesh,
        in_specs=placed,
        out_specs=(P("dp", ("kv", "tp")), P(("dp", "kv"), "tp", None, None)),
        check_vma=False,
    )
```

profile of v0, /device:TPU:0, one launch (start us, length us, event | category | flops | bytes accessed | tf_op | source)
XLA Modules:
  0.0 167.2 jit_solution(12161936013294554536)
XLA Ops:
  7.2 0.0 copy-start
  7.2 0.0 all-reduce.3.cloned.1.call-start
  7.2 0.0 copy-start.4
  7.2 16.0 %all_gather.9 = bf16[8,4096]{1,0:T(8,128)(2,1)S(1)} all-gather(bf16[8,512]{1,0:T(8,128)(2,1)} %param.16), channel_id=1, replica_groups=mesh['dp'=4,'kv'=4,'tp'=2] {'kv','tp'}, dimensions={1}, use_global_device_ids=true | all-gather | bytes 73728 | tf_op jit(solution)/shard_map/all_gather | solution.py:43
  23.3 0.0 copy-done
  23.3 0.6 fusion.7
  23.9 0.0 copy-done.4
  23.9 0.0 copy-start.2
  23.9 0.7 fusion.6
  24.6 2.6 %fusion.5 = bf16[8,1792]{1,0:T(8,128)(2,1)S(1)} fusion(bf16[8,1792]{1,0:T(8,128)(2,1)S(1)} %fusion.6, bf16[8,4096]{1,0:T(8,128)(2,1)S(1)} %all_gather.9, bf16[4096,256]{0,1:T(8,128)(2,1)} %bitcast.60), kind=kOutput, calls=%fused_computation.11 | convolution fusion | flops 16779264 | bytes 2166784 | tf_op jit(solution)/shard_map/dot_general | solution.py:16
  27.2 0.0 copy-done.2
  27.2 0.0 copy-start.3
  27.2 1.2 fusion.4
  28.4 1.0 copy-done.3
  29.4 0.0 copy-start.7
  29.4 1.2 fusion.3
  30.6 10.1 %all_to_all.12 = bf16[4,2,1792]{2,1,0:T(2,128)(2,1)S(1)} all-to-all(bf16[4,2,1792]{2,1,0:T(2,128)(2,1)S(1)} %all_to_all.8), channel_id=1, replica_groups=mesh['dp'=4,'kv'=4,'tp'=2] {'kv'}, dimensions={0} | all-to-all | bytes 57344 | tf_op jit(solution)/shard_map/all_to_all | solution.py:46
  40.7 0.1 reshape.138
  40.8 0.1 reshape.134
  40.9 0.1 reshape.136
  41.0 0.1 reshape.132
  41.1 0.1 reshape.137
  41.2 0.1 reshape.133
  41.3 0.1 mul.135
  41.4 0.1 reshape.140
  41.4 0.0 copy-done.7
  41.5 1.9 %multiply_add_fusion = f32[2,8,128,256]{3,2,1,0:T(8,128)S(1)} fusion(f32[2,8,128,256]{3,2,1,0:T(8,128)} %param.23, f32[2,8,256]{2,1,0:T(8,128)S(1)} %reshape.134, f32[2,8,128]{2,1,0:T(8,128)S(1)} %reshape.133, f32[2,8,128]{2,1,0:T(8,128)S(1)} %fusion.16), kind=kLoop, calls=%fused_computation.3 | loop fusion | flops 1572864 | bytes 4227072 | tf_op jit(solution)/shard_map/add | solution.py:65
  43.4 0.0 copy-start.1
  43.4 0.0 copy-start.6
  43.4 0.0 copy-start.5
  43.4 1.3 copy-done.1
  44.7 1.1 fusion.20
  45.8 0.1 fusion.10
  45.9 0.1 reshape.139
  46.0 0.1 reshape.135
  46.1 0.0 copy-done.6
  46.1 0.1 fusion.13
  46.2 14.0 %all_gather.10 = bf16[8,2,2048]{2,1,0:T(2,128)(2,1)S(1)} all-gather(bf16[1,2,2048]{2,1,0:T(2,128)(2,1)S(1)} %reshape.129), channel_id=1, replica_groups=mesh['dp'=4,'kv'=4,'tp'=2] {'kv','tp'}, dimensions={0}, use_global_device_ids=true | all-gather | bytes 73728 | tf_op jit(solution)/shard_map/all_gather | solution.py:75
  60.3 0.0 copy-done.5
  60.3 0.0 copy-start.8
  60.3 0.0 copy-start.9
  60.3 3.0 %fusion.19 = (f32[8]{0:T(128)S(1)}, f32[8]{0:T(128)S(1)}, f32[8,512]{1,0:T(8,128)S(1)}) fusion(bf16[8,2048,2]{1,0,2:T(8,128)(2,1)S(1)} %dot_general.38, bf16[2,2048,512]{2,1,0:T(8,128)(2,1)} %bitcast.56, bf16[8,512]{1,0:T(8,128)(2,1)S(1)} %copy-done.5), kind=kOutput, calls=%fused_computation.45 | convolution fusion | flops 33578992 | bytes 4284480 | tf_op jit(solution)/shard_map/atsc,tcd->asd/dot_general | solution.py:82
  63.3 14.2 %all-reduce = (f32[8,1]{0,1:T(1,128)S(1)}, f32[8,1]{0,1:T(1,128)S(1)}) all-reduce(f32[8,1]{0,1:T(1,128)S(1)} %bitcast.69, f32[8,1]{0,1:T(1,128)S(1)} %bitcast.68), channel_id=1, replica_groups=mesh['dp'=4,'kv'=4,'tp'=2] {'kv','tp'}, use_global_device_ids=true, to_apply=%region_4.5 | all-reduce | flops 16 | bytes 128 | tf_op jit(solution)/shard_map/psum | solution.py:87
  77.6 0.0 copy-done.8
  77.6 0.0 copy-done.9
  77.6 0.1 add_convert_fusion.1
  77.7 14.0 %all_gather.11 = bf16[8,4096]{1,0:T(8,128)(2,1)S(1)} all-gather(bf16[8,512]{1,0:T(8,128)(2,1)S(1)} %add_convert_fusion.1), channel_id=1, replica_groups=mesh['dp'=4,'kv'=4,'tp'=2] {'kv','tp'}, dimensions={1}, use_global_device_ids=true | all-gather | bytes 73728 | tf_op jit(solution)/shard_map/all_gather | solution.py:97
  91.6 0.0 copy-start.10
  91.6 0.0 copy-start.11
  91.6 13.5 %fusion.8 = f32[8,4096]{1,0:T(8,128)} fusion(bf16[2048,4096]{1,0:T(8,128)(2,1)} %param.29, bf16[8,4096]{1,0:T(8,128)(2,1)S(1)} %all_gather.11, bf16[4096,2048]{1,0:T(8,128)(2,1)} %param.28), kind=kOutput, calls=%fused_computation.16 | convolution fusion | flops 268484608 | bytes 33751040 | tf_op jit(solution)/shard_map/dot_general | solution.py:100
  105.2 0.0 all-reduce.3.cloned.1.call-update
  105.2 53.4 %all-reduce.3.cloned.1.call-done = f32[8,4096]{1,0:T(8,128)} async-done(((f32[8,4096]{1,0:T(8,128)}), f32[8,4096]{1,0:T(8,128)}) %all-reduce.3.cloned.1.call-update) | async-done | bytes 131088 | tf_op jit(solution)/shard_map/psum | solution.py:101
  158.5 1.1 fusion.18
  159.6 0.0 copy-done.10
  159.6 0.0 copy-done.11
  159.6 0.7 add_convert_fusion
  (17 shorter events, 0.3 us)
Async XLA Ops:
  7.2 16.1 %copy-start = (bf16[4096,8,32]{0,2,1:T(8,128)(2,1)S(1)}, bf16[4096,8,32]{0,2,1:T(8,128)(2,1)}, u32[]{:S(2)}) copy-start(bf16[4096,8,32]{0,2,1:T(8,128)(2,1)} %param.17) | copy-start | bytes 6291460
  7.2 151.4 %all-reduce.3.cloned.1.call-start = ((), (), s32[]{:S(2)}) async-start(), calls=%async_computation.1 | async-start | bytes 262144 | tf_op jit(solution)/shard_map/psum | solution.py:101
  7.2 16.7 %copy-start.4 = (bf16[4096,8,32]{0,2,1:T(8,128)(2,1)S(1)}, bf16[4096,8,32]{0,2,1:T(8,128)(2,1)}, u32[]{:S(2)}) copy-start(bf16[4096,8,32]{0,2,1:T(8,128)(2,1)} %param.18) | copy-start | bytes 6291460
  23.9 3.2 %copy-start.2 = (bf16[4096,8,64]{0,2,1:T(8,128)(2,1)S(1)}, bf16[4096,8,64]{0,2,1:T(8,128)(2,1)}, u32[]{:S(2)}) copy-start(bf16[4096,8,64]{0,2,1:T(8,128)(2,1)} %param.19) | copy-start | bytes 12582916
  27.2 2.2 %copy-start.3 = (bf16[4096,8,64]{0,2,1:T(8,128)(2,1)S(1)}, bf16[4096,8,64]{0,2,1:T(8,128)(2,1)}, u32[]{:S(2)}) copy-start(bf16[4096,8,64]{0,2,1:T(8,128)(2,1)} %param.20) | copy-start | bytes 12582916
  29.4 12.1 %copy-start.7 = (f32[8,128]{1,0:T(8,128)S(1)}, f32[8,128]{1,0:T(8,128)}, u32[]{:S(2)}) copy-start(f32[8,128]{1,0:T(8,128)} %param.22) | copy-start | bytes 12292
  43.4 1.3 copy-start.1
  43.4 2.7 %copy-start.6 = (f32[8,256]{1,0:T(8,128)S(1)}, f32[8,256]{1,0:T(8,128)}, u32[]{:S(2)}) copy-start(f32[8,256]{1,0:T(8,128)} %param.24) | copy-start | bytes 24580
  43.4 16.9 %copy-start.5 = (bf16[8,512]{1,0:T(8,128)(2,1)S(1)}, bf16[8,512]{1,0:T(8,128)(2,1)}, u32[]{:S(2)}) copy-start(bf16[8,512]{1,0:T(8,128)(2,1)} %param.16) | copy-start | bytes 24580
  60.3 17.3 %copy-start.8 = (f32[512]{0:T(512)S(1)}, f32[512]{0:T(512)}, u32[]{:S(2)}) copy-start(f32[512]{0:T(512)} %param.27) | copy-start | bytes 6148
  60.3 17.3 %copy-start.9 = (f32[512]{0:T(512)S(1)}, f32[512]{0:T(512)}, u32[]{:S(2)}) copy-start(f32[512]{0:T(512)} %param.26) | copy-start | bytes 6148
  91.6 68.0 %copy-start.10 = (f32[512]{0:T(512)S(1)}, f32[512]{0:T(512)}, u32[]{:S(2)}) copy-start(f32[512]{0:T(512)} %param.31) | copy-start | bytes 6148
  91.6 68.0 %copy-start.11 = (f32[512]{0:T(512)S(1)}, f32[512]{0:T(512)}, u32[]{:S(2)}) copy-start(f32[512]{0:T(512)} %param.30) | copy-start | bytes 6148
Sparse Core Ops, SparseCore 0:
  105.3 53.1 all-reduce.2
where the time goes:
time: 167 us
  blocking collectives  68.3 us (41%)
  waiting for transfers between devices  53.4 us (32%)
  matrix products  23.9 us (14%)
  between operations  14.2 us (9%)
  other arithmetic  4 us (2%)
  local copies, waits for them, and re-layouts  3.36 us (2%)
    psum x1, waiting for transfers between devices, body(): mixer_all = lax.psum(mixer_term, ('kv', 'tp'))  53.4 us
    all_gather x1, blocking collectives, body(): whole = lax.all_gather(tokens, ('kv', 'tp'), axis=1, tiled=True)  16 us
    psum x1, blocking collectives, body(): lax.psum((jnp.sum(residual_one, axis=-1, keepdims=True), jnp.sum(residual...  14.2 us
    all_gather x1, blocking collectives, body(): lax.all_gather(attended.reshape(1, seq_count, flat_width), ('kv', 'tp'),...  14 us
    all_gather x1, blocking collectives, body(): normed = lax.all_gather(normed_own, ('kv', 'tp'), axis=1, tiled=True)  14 us
    dot_general x1, matrix products, body(): jnp.dot(hidden, down_weight, preferred_element_type=jnp.float32)  13.5 us
    all_to_all x1, blocking collectives, body(): lax.all_to_all(packed, 'kv', split_axis=0, concat_axis=0, tiled=True)  10.1 us
    dot_general x5, matrix products, project_flat(): jnp.dot(inputs, flattened, preferred_element_type=jnp.float32)  6.25 us
  transfers between devices with their start and end apart: 1, of which 1 were waited for; matrix products, arithmetic and copies ran while one was open for 0% of the time, Pallas kernels for 0%

commit v1 on v0

--- a/solution.py
+++ b/solution.py
@@ -98,7 +98,7 @@
     lifted = jnp.dot(normed, up_weight, preferred_element_type=jnp.float32)
     hidden = jnp.square(jax.nn.relu(lifted)).astype(jnp.bfloat16)
     mixer_term = jnp.dot(hidden, down_weight, preferred_element_type=jnp.float32)
-    mixer_all = lax.psum(mixer_term, ("kv", "tp"))
+    mixer_all = jnp.sum(lax.all_gather(mixer_term, ("kv", "tp")), axis=0)
     residual_two = ALPHA * normed.astype(jnp.float32) + mixer_all
     average = jnp.sum(residual_two, axis=-1, keepdims=True) / D
     spread = jnp.sum(residual_two * residual_two, axis=-1, keepdims=True) / D - average * average

time: 167 us -> 135 us (0.81)
  waiting for transfers between devices: 53.4 us -> 20.6 us
    psum x1 -> x0, waiting for transfers between devices: 53.4 us -> none  [body(): mixer_all = lax.psum(mixer_term, ('kv', 'tp'))]
    all_gather x0 -> x1, waiting for transfers between devices: none -> 20.6 us  [body(): mixer_all = jnp.sum(lax.all_gather(mixer_term, ('kv', 'tp')), axis=0)]
where the time goes in v1:
time: 135 us
  blocking collectives  68.3 us (51%)
  matrix products  23.9 us (18%)
  waiting for transfers between devices  20.6 us (15%)
  between operations  14.2 us (11%)
  other arithmetic  4.38 us (3%)
  local copies, waits for them, and re-layouts  3.36 us (2%)
    all_gather x1, waiting for transfers between devices, body(): mixer_all = jnp.sum(lax.all_gather(mixer_term, ('kv', 'tp')), axis=0)  20.6 us
    all_gather x1, blocking collectives, body(): whole = lax.all_gather(tokens, ('kv', 'tp'), axis=1, tiled=True)  16 us
    psum x1, blocking collectives, body(): lax.psum((jnp.sum(residual_one, axis=-1, keepdims=True), jnp.sum(residual...  14.2 us
    all_gather x1, blocking collectives, body(): lax.all_gather(attended.reshape(1, seq_count, flat_width), ('kv', 'tp'),...  14 us
    all_gather x1, blocking collectives, body(): normed = lax.all_gather(normed_own, ('kv', 'tp'), axis=1, tiled=True)  14 us
    dot_general x1, matrix products, body(): jnp.dot(hidden, down_weight, preferred_element_type=jnp.float32)  13.5 us
    all_to_all x1, blocking collectives, body(): lax.all_to_all(packed, 'kv', split_axis=0, concat_axis=0, tiled=True)  10.1 us
    dot_general x5, matrix products, project_flat(): jnp.dot(inputs, flattened, preferred_element_type=jnp.float32)  6.25 us
  transfers between devices with their start and end apart: 1, of which 1 were waited for; matrix products, arithmetic and copies ran while one was open for 0% of the time, Pallas kernels for 0%

profile of v1, /device:TPU:0, one launch (start us, length us, event | category | flops | bytes accessed | tf_op | source)
XLA Modules:
  0.0 134.8 jit_solution(10288028128793730151)
XLA Ops:
  7.2 0.0 copy-start
  7.2 0.0 all-gather.3.cloned.1.call-start
  7.2 0.0 copy-start.4
  7.2 16.0 %all_gather.15 = bf16[8,4096]{1,0:T(8,128)(2,1)S(1)} all-gather(bf16[8,512]{1,0:T(8,128)(2,1)} %param.16), channel_id=1, replica_groups=mesh['dp'=4,'kv'=4,'tp'=2] {'kv','tp'}, dimensions={1}, use_global_device_ids=true | all-gather | bytes 73728 | tf_op jit(solution)/shard_map/all_gather | solution.py:43
  23.3 0.0 copy-done
  23.3 0.6 fusion.7
  23.9 0.0 copy-done.4
  23.9 0.0 copy-start.2
  23.9 0.7 fusion.6
  24.6 2.6 %fusion.5 = bf16[8,1792]{1,0:T(8,128)(2,1)S(1)} fusion(bf16[8,1792]{1,0:T(8,128)(2,1)S(1)} %fusion.6, bf16[8,4096]{1,0:T(8,128)(2,1)S(1)} %all_gather.15, bf16[4096,256]{0,1:T(8,128)(2,1)} %bitcast.62), kind=kOutput, calls=%fused_computation.11 | convolution fusion | flops 16779264 | bytes 2166784 | tf_op jit(solution)/shard_map/dot_general | solution.py:16
  27.2 0.0 copy-done.2
  27.2 0.0 copy-start.3
  27.2 1.2 fusion.4
  28.4 1.0 copy-done.3
  29.4 0.0 copy-start.7
  29.4 1.2 fusion.3
  30.6 10.1 %all_to_all.12 = bf16[4,2,1792]{2,1,0:T(2,128)(2,1)S(1)} all-to-all(bf16[4,2,1792]{2,1,0:T(2,128)(2,1)S(1)} %all_to_all.8), channel_id=1, replica_groups=mesh['dp'=4,'kv'=4,'tp'=2] {'kv'}, dimensions={0} | all-to-all | bytes 57344 | tf_op jit(solution)/shard_map/all_to_all | solution.py:46
  40.7 0.1 reshape.138
  40.8 0.1 reshape.134
  40.9 0.1 reshape.136
  41.0 0.1 reshape.132
  41.1 0.1 reshape.137
  41.2 0.1 reshape.133
  41.3 0.1 mul.135
  41.4 0.1 reshape.141
  41.4 0.0 copy-done.7
  41.5 1.9 %multiply_add_fusion = f32[2,8,128,256]{3,2,1,0:T(8,128)S(1)} fusion(f32[2,8,128,256]{3,2,1,0:T(8,128)} %param.23, f32[2,8,256]{2,1,0:T(8,128)S(1)} %reshape.134, f32[2,8,128]{2,1,0:T(8,128)S(1)} %reshape.133, f32[2,8,128]{2,1,0:T(8,128)S(1)} %fusion.16), kind=kLoop, calls=%fused_computation.3 | loop fusion | flops 1572864 | bytes 4227072 | tf_op jit(solution)/shard_map/add | solution.py:65
  43.4 0.0 copy-start.1
  43.4 0.0 copy-start.6
  43.4 0.0 copy-start.5
  43.4 1.3 copy-done.1
  44.7 1.1 fusion.20
  45.8 0.1 fusion.10
  45.9 0.1 reshape.139
  46.0 0.1 reshape.135
  46.1 0.0 copy-done.6
  46.1 0.1 fusion.13
  46.2 14.0 %all_gather.16 = bf16[8,2,2048]{2,1,0:T(2,128)(2,1)S(1)} all-gather(bf16[1,2,2048]{2,1,0:T(2,128)(2,1)S(1)} %reshape.129), channel_id=1, replica_groups=mesh['dp'=4,'kv'=4,'tp'=2] {'kv','tp'}, dimensions={0}, use_global_device_ids=true | all-gather | bytes 73728 | tf_op jit(solution)/shard_map/all_gather | solution.py:75
  60.3 0.0 copy-done.5
  60.3 0.0 copy-start.8
  60.3 0.0 copy-start.9
  60.3 3.0 %fusion.19 = (f32[8]{0:T(128)S(1)}, f32[8]{0:T(128)S(1)}, f32[8,512]{1,0:T(8,128)S(1)}) fusion(bf16[8,2048,2]{1,0,2:T(8,128)(2,1)S(1)} %dot_general.38, bf16[2,2048,512]{2,1,0:T(8,128)(2,1)} %bitcast.58, bf16[8,512]{1,0:T(8,128)(2,1)S(1)} %copy-done.5), kind=kOutput, calls=%fused_computation.46 | convolution fusion | flops 33578992 | bytes 4284480 | tf_op jit(solution)/shard_map/atsc,tcd->asd/dot_general | solution.py:82
  63.3 14.2 %all-reduce = (f32[8,1]{0,1:T(1,128)S(1)}, f32[8,1]{0,1:T(1,128)S(1)}) all-reduce(f32[8,1]{0,1:T(1,128)S(1)} %bitcast.71, f32[8,1]{0,1:T(1,128)S(1)} %bitcast.70), channel_id=1, replica_groups=mesh['dp'=4,'kv'=4,'tp'=2] {'kv','tp'}, use_global_device_ids=true, to_apply=%region_4.5 | all-reduce | flops 16 | bytes 128 | tf_op jit(solution)/shard_map/psum | solution.py:87
  77.6 0.0 copy-done.8
  77.6 0.0 copy-done.9
  77.6 0.1 add_convert_fusion.1
  77.7 14.0 %all_gather.17 = bf16[8,4096]{1,0:T(8,128)(2,1)S(1)} all-gather(bf16[8,512]{1,0:T(8,128)(2,1)S(1)} %add_convert_fusion.1), channel_id=1, replica_groups=mesh['dp'=4,'kv'=4,'tp'=2] {'kv','tp'}, dimensions={1}, use_global_device_ids=true | all-gather | bytes 73728 | tf_op jit(solution)/shard_map/all_gather | solution.py:97
  91.6 0.0 copy-start.10
  91.6 0.0 copy-start.11
  91.6 13.5 %fusion.8 = f32[8,4096]{1,0:T(8,128)} fusion(bf16[2048,4096]{1,0:T(8,128)(2,1)} %param.29, bf16[8,4096]{1,0:T(8,128)(2,1)S(1)} %all_gather.17, bf16[4096,2048]{1,0:T(8,128)(2,1)} %param.28), kind=kOutput, calls=%fused_computation.17 | convolution fusion | flops 268484608 | bytes 33751040 | tf_op jit(solution)/shard_map/dot_general | solution.py:100
  105.2 0.0 all-gather.3.cloned.1.call-update
  105.2 20.6 %all-gather.3.cloned.1.call-done = f32[64,4096]{1,0:T(8,128)} async-done(((f32[8,4096]{1,0:T(8,128)}), f32[64,4096]{1,0:T(8,128)}) %all-gather.3.cloned.1.call-update) | async-done | bytes 1048592 | tf_op jit(solution)/shard_map/all_gather | solution.py:101
  125.8 1.3 bitcast_reduce_fusion
  127.1 0.2 fusion.18
  127.3 0.0 copy-done.10
  127.3 0.0 copy-done.11
  127.3 0.7 add_convert_fusion
  (17 shorter events, 0.3 us)
Async XLA Ops:
  7.2 16.1 %copy-start = (bf16[4096,8,32]{0,2,1:T(8,128)(2,1)S(1)}, bf16[4096,8,32]{0,2,1:T(8,128)(2,1)}, u32[]{:S(2)}) copy-start(bf16[4096,8,32]{0,2,1:T(8,128)(2,1)} %param.17) | copy-start | bytes 6291460
  7.2 118.6 %all-gather.3.cloned.1.call-start = ((), (), s32[]{:S(2)}) async-start(), calls=%async_computation.1 | async-start | bytes 1179648 | tf_op jit(solution)/shard_map/all_gather | solution.py:101
  7.2 16.7 %copy-start.4 = (bf16[4096,8,32]{0,2,1:T(8,128)(2,1)S(1)}, bf16[4096,8,32]{0,2,1:T(8,128)(2,1)}, u32[]{:S(2)}) copy-start(bf16[4096,8,32]{0,2,1:T(8,128)(2,1)} %param.18) | copy-start | bytes 6291460
  23.9 3.2 %copy-start.2 = (bf16[4096,8,64]{0,2,1:T(8,128)(2,1)S(1)}, bf16[4096,8,64]{0,2,1:T(8,128)(2,1)}, u32[]{:S(2)}) copy-start(bf16[4096,8,64]{0,2,1:T(8,128)(2,1)} %param.19) | copy-start | bytes 12582916
  27.2 2.2 %copy-start.3 = (bf16[4096,8,64]{0,2,1:T(8,128)(2,1)S(1)}, bf16[4096,8,64]{0,2,1:T(8,128)(2,1)}, u32[]{:S(2)}) copy-start(bf16[4096,8,64]{0,2,1:T(8,128)(2,1)} %param.20) | copy-start | bytes 12582916
  29.4 12.1 %copy-start.7 = (f32[8,128]{1,0:T(8,128)S(1)}, f32[8,128]{1,0:T(8,128)}, u32[]{:S(2)}) copy-start(f32[8,128]{1,0:T(8,128)} %param.22) | copy-start | bytes 12292
  43.4 1.3 copy-start.1
  43.4 2.7 %copy-start.6 = (f32[8,256]{1,0:T(8,128)S(1)}, f32[8,256]{1,0:T(8,128)}, u32[]{:S(2)}) copy-start(f32[8,256]{1,0:T(8,128)} %param.24) | copy-start | bytes 24580
  43.4 16.9 %copy-start.5 = (bf16[8,512]{1,0:T(8,128)(2,1)S(1)}, bf16[8,512]{1,0:T(8,128)(2,1)}, u32[]{:S(2)}) copy-start(bf16[8,512]{1,0:T(8,128)(2,1)} %param.16) | copy-start | bytes 24580
  60.3 17.3 %copy-start.8 = (f32[512]{0:T(512)S(1)}, f32[512]{0:T(512)}, u32[]{:S(2)}) copy-start(f32[512]{0:T(512)} %param.27) | copy-start | bytes 6148
  60.3 17.3 %copy-start.9 = (f32[512]{0:T(512)S(1)}, f32[512]{0:T(512)}, u32[]{:S(2)}) copy-start(f32[512]{0:T(512)} %param.26) | copy-start | bytes 6148
  91.6 35.6 %copy-start.10 = (f32[512]{0:T(512)S(1)}, f32[512]{0:T(512)}, u32[]{:S(2)}) copy-start(f32[512]{0:T(512)} %param.31) | copy-start | bytes 6148
  91.6 35.6 %copy-start.11 = (f32[512]{0:T(512)S(1)}, f32[512]{0:T(512)}, u32[]{:S(2)}) copy-start(f32[512]{0:T(512)} %param.30) | copy-start | bytes 6148
Sparse Core Ops, SparseCore 0:
  105.3 20.4 all-gather.2
